TPU v7x, 32 devices: a whole 2x2x4 slice. The times are simulated.
32 devices in a mesh: sp: 4 (over y, core), dp: 8 (over z, x).
Axes of the slice: x: 2, y: 2, z: 4, core: 2. Of those that a mesh axis runs over, the one named last changes fastest.
Arguments:
- q_latent: bfloat16 [8, 512, 512], P('dp', 'sp'), may hold values from -70 to 70
- kv_latent: bfloat16 [8, 512, 512], P('dp', 'sp'), may hold values from -70 to 70
- rope_key: bfloat16 [8, 512, 64], P('dp', 'sp'), may hold values from -370 to 370
- w_query: bfloat16 [512, 3072], P(None, 'dp'), may hold values from -0.25 to 0.25
- w_keyval: bfloat16 [512, 4096], P(None, 'sp'), may hold values from -0.25 to 0.25
- w_out: bfloat16 [2048, 2048], replicated, may hold values from -0.125 to 0.125
- query_gain: bfloat16 [512], replicated, may hold values from 0.099609375 to 1.8984375
- latent_gain: bfloat16 [512], replicated, may hold values from 0.099609375 to 1.8984375
- out_gain: bfloat16 [2048], replicated, may hold values from 0.099609375 to 1.8984375
Outputs:
- output: bfloat16 [8, 512, 2048], P('dp', 'sp')
All inputs are finite; a program needn't handle non-finite values.
Results may differ from a plain program's by a relative error of at most 0.03.
The roundings to bfloat16 on the way count: a program that leaves them out, or rounds other values in their place, can miss the bound.
Values may be sent and summed in bfloat16 or wider, within the bound.
A program may use at most 64 MiB of HBM per device.

v0:
```python
import jax
import jax.numpy as jnp
from jax import lax
from jax.sharding import PartitionSpec as P

H = 16
NOPE = 128
ROPE = 64
VDIM = 128


def normalize(row_values, gain_vector):
    widened = row_values.astype(jnp.float32)
    return (
        widened
        * lax.rsqrt(jnp.mean(widened * widened, axis=-1, keepdims=True) + 1e-05)
        * gain_vector.astype(jnp.float32)
    )


def angles_for(positions, rope_width):
    half_width = rope_width // 2
    inverse = 10000.0 ** (-jnp.arange(half_width, dtype=jnp.float32) / half_width)
    return positions.astype(jnp.float32)[:, None] * inverse[None, :]


def turn(vectors, angles):
    half_width = vectors.shape[-1] // 2
    cosine = jnp.cos(angles)
    sine_value = jnp.sin(angles)
    low_half = vectors[..., :half_width]
    high_half = vectors[..., half_width:]
    return jnp.concatenate(
        [low_half * cosine - high_half * sine_value, high_half * cosine + low_half * sine_value],
        axis=-1,
    )


def attend(query_head, keyval_head, rope_all):
    length = query_head.shape[0]
    local_heads = query_head.shape[1] // (NOPE + ROPE)
    query_three = query_head.reshape(length, local_heads, NOPE + ROPE)
    keyval_three = keyval_head.reshape(length, local_heads, NOPE + VDIM)
    block_rows = min(512, length)
    score_scale = (NOPE + ROPE) ** (-0.5)
    pieces = []
    for block_index in range(length // block_rows):
        block_start = block_index * block_rows
        block_stop = block_start + block_rows
        query_block = query_three[block_start:block_stop]
        scores = jnp.einsum(
            "qhd,khd->hqk",
            query_block[..., :NOPE],
            keyval_three[:block_stop, :, :NOPE],
            preferred_element_type=jnp.float32,
        )
        scores = scores + jnp.einsum(
            "qhr,kr->hqk",
            query_block[..., NOPE:],
            rope_all[:block_stop],
            preferred_element_type=jnp.float32,
        )
        scores = scores * score_scale
        allowed = jnp.arange(block_stop)[None, :] <= (block_start + jnp.arange(block_rows))[:, None]
        scores = jnp.where(allowed[None], scores, -jnp.inf)
        row_top = jnp.max(scores, axis=-1, keepdims=True)
        exponent = jnp.exp(scores - row_top)
        row_total = jnp.sum(exponent, axis=-1)
        summed = jnp.einsum(
            "hqk,khd->qhd",
            exponent.astype(jnp.bfloat16),
            keyval_three[:block_stop, :, NOPE:],
            preferred_element_type=jnp.float32,
        )
        pieces.append((summed / jnp.transpose(row_total)[:, :, None]).astype(jnp.bfloat16))
    return jnp.concatenate(pieces, axis=0).reshape(length, local_heads * VDIM)


def per_device(
    q_latent, kv_latent, rope_key, w_query, w_keyval, w_out, query_gain, latent_gain, out_gain
):
    tokens_here = q_latent.shape[1]
    offset = lax.axis_index("sp") * tokens_here
    positions = offset + jnp.arange(tokens_here, dtype=jnp.int32)
    angles = angles_for(positions, ROPE)
    query_norm = normalize(q_latent[0], query_gain).astype(jnp.bfloat16)
    query_raw = jnp.dot(
        query_norm,
        lax.all_gather(w_query, "dp", axis=1, tiled=True),
        preferred_element_type=jnp.float32,
    )
    query_raw = query_raw.reshape(tokens_here, H, NOPE + ROPE)
    queries = jnp.concatenate(
        [query_raw[..., :NOPE], turn(query_raw[..., NOPE:], angles[:, None, :])], axis=-1
    )
    queries = queries.astype(jnp.bfloat16).reshape(tokens_here, H * (NOPE + ROPE))
    latent_norm = normalize(kv_latent[0], latent_gain).astype(jnp.bfloat16)
    rope_turned = turn(rope_key[0].astype(jnp.float32), angles).astype(jnp.bfloat16)
    query_head = lax.all_to_all(queries, "sp", split_axis=1, concat_axis=0, tiled=True)
    latent_all, rope_all = (
        lax.all_gather(latent_norm, "sp", axis=0, tiled=True),
        lax.all_gather(rope_turned, "sp", axis=0, tiled=True),
    )
    keyval_head = jnp.dot(latent_all, w_keyval, preferred_element_type=jnp.float32).astype(
        jnp.bfloat16
    )
    attended = attend(query_head, keyval_head, rope_all)
    returned = lax.all_to_all(attended, "sp", split_axis=0, concat_axis=1, tiled=True)
    mixed_norm = normalize(returned, out_gain).astype(jnp.bfloat16)
    result = jnp.dot(mixed_norm, w_out, preferred_element_type=jnp.float32).astype(jnp.bfloat16)
    return result[None]


def solution(mesh):
    in_specs = (
        P("dp", "sp", None),
        P("dp", "sp", None),
        P("dp", "sp", None),
        P(None, "dp"),
        P(None, "sp"),
        P(),
        P(),
        P(),
        P(),
    )
    out_specs = P("dp", "sp", None)
    return jax.shard_map(
        per_device, mesh=mesh, in_specs=in_specs, out_specs=out_specs, check_vma=False
    )
```

profile of v0, /device:TPU:1, one launch (start us, length us, event | category | flops | bytes accessed | tf_op | source)
XLA Modules:
  0.0 131.7 jit_solution(3271215150385826949)
XLA Ops:
  6.5 0.7 all-gather.2.cloned.1.call-update
  7.3 0.7 convert_element_type.83
  7.9 0.7 convert_element_type.79
  8.6 1.0 fusion.23
  9.7 1.0 fusion.26
  10.7 1.0 fusion.28
  11.7 8.5 %all_gather.9 = bf16[512,512]{1,0:T(8,128)(2,1)S(1)} all-gather(bf16[128,512]{1,0:T(8,128)(2,1)S(1)} %fusion.28), channel_id=1, replica_groups=mesh['sp'=4,'dp'=8] {'sp'}, dimensions={0}, use_global_device_ids=true | all-gather | bytes 655360 | tf_op jit(solution)/shard_map/all_gather | solution.py:101
  20.2 0.7 bitcast_convert_fusion
  21.0 0.1 subtract_convert_fusion.1
  21.1 52.3 %all-gather.2.cloned.1.call-done = bf16[512,3072]{1,0:T(8,128)(2,1)} async-done(((bf16[512,384]{1,0:T(8,128)(2,1)}), bf16[512,3072]{1,0:T(8,128)(2,1)}) %all-gather.2.cloned.1.call-update) | async-done | bytes 3145744 | tf_op jit(solution)/shard_map/all_gather | solution.py:89
  73.4 4.7 %copy.23 = bf16[3072,512]{1,0:T(8,128)(2,1)} copy(bf16[3072,512]{0,1:T(8,128)(2,1)} %bitcast.53) | data formatting | bytes 6291456 | tf_op jit(solution)/shard_map/dot_general | solution.py:87
  78.1 2.9 %fusion.31 = f32[128,16,192]{0,2,1:T(8,128)S(1)} fusion(bf16[16,192,512]{2,1,0:T(8,128)(2,1)} %bitcast.52, bf16[1,128,512]{2,1,0:T(8,128)(2,1)S(1)} %copy-done.2, f32[512]{0:T(512)S(1)} %convert_element_type.83, f32[128]{0:T(128)S(1)} %add_rsqrt_fusion.1), kind=kOutput, calls=%fused_computation.39 | convolution fusion | flops 402915328 | bytes 4852224 | tf_op jit(solution)/shard_map/dot_general | solution.py:87
  81.2 1.0 pad_maximum_fusion
  82.2 4.9 %all-to-all-start = ((bf16[128,4,768]{0,2,1:T(8,128)(2,1)}), bf16[128,4,768]{0,2,1:T(8,128)(2,1)S(1)}, u32[]{:S(2)}, u32[]{:S(2)}) async-start(bf16[128,4,768]{0,2,1:T(8,128)(2,1)} %bitcast.6), calls=%async_computation | async-start | bytes 1572864 | tf_op jit(solution)/shard_map/all_to_all | solution.py:99
  87.1 1.7 %convolution_convert_fusion.1 = bf16[512,1024]{1,0:T(8,128)(2,1)} fusion(bf16[512,512]{1,0:T(8,128)(2,1)S(1)} %all_gather.9, bf16[512,1024]{1,0:T(8,128)(2,1)S(1)} %copy-done), kind=kOutput, calls=%fused_computation.10 | convolution fusion | flops 537395200 | bytes 2621440 | tf_op jit(solution)/shard_map/dot_general | solution.py:104
  88.8 1.9 %reshape.144 = bf16[512,4,256]{2,1,0:T(4,128)(2,1)S(1)} reshape(bf16[512,1024]{1,0:T(8,128)(2,1)} %convolution_convert_fusion.1) | data formatting | bytes 2097152 | tf_op jit(solution)/shard_map/reshape | solution.py:43
  90.6 9.1 %all_gather.11 = bf16[512,64]{0,1:T(8,128)(2,1)S(1)} all-gather(bf16[128,64]{0,1:T(8,128)(2,1)S(1)} %pad_maximum_fusion.1), channel_id=1, replica_groups=mesh['sp'=4,'dp'=8] {'sp'}, dimensions={0}, use_global_device_ids=true | all-gather | bytes 81920 | tf_op jit(solution)/shard_map/all_gather | solution.py:102
  99.7 0.8 iota_compare_fusion
  100.5 1.2 fusion.36
  101.7 0.6 copy.24
  102.3 0.3 reshape.145
  102.6 0.7 fusion.19
  103.3 1.2 fusion.37
  104.5 0.6 fusion.2
  105.1 0.5 copy-done.3
  105.5 0.8 fusion.14
  106.4 0.9 copy.28
  107.3 3.6 %all-to-all-start.1 = ((bf16[4,128,512]{1,2,0:T(8,128)(2,1)}), bf16[4,128,512]{1,2,0:T(8,128)(2,1)S(1)}, u32[]{:S(2)}, u32[]{:S(2)}) async-start(bf16[4,128,512]{1,2,0:T(8,128)(2,1)} %copy.28), calls=%async_computation.1 | async-start | bytes 1048576 | tf_op jit(solution)/shard_map/all_to_all | solution.py:108
  110.9 7.8 %all-to-all-done.1 = bf16[4,128,512]{1,2,0:T(8,128)(2,1)S(1)} async-done(((bf16[4,128,512]{1,2,0:T(8,128)(2,1)}), bf16[4,128,512]{1,2,0:T(8,128)(2,1)S(1)}, u32[]{:S(2)}, u32[]{:S(2)}) %all-to-all-start.1) | async-done | bytes 524320 | tf_op jit(solution)/shard_map/all_to_all | solution.py:108
  118.8 0.3 multiply_reduce_fusion
  119.1 0.3 fusion.18
  119.4 5.5 %fusion.4 = bf16[1,128,2048]{2,1,0:T(8,128)(2,1)} fusion(bf16[128,2048]{0,1:T(8,128)(2,1)S(1)} %fusion.18, bf16[2048,2048]{1,0:T(8,128)(2,1)} %param.14), kind=kOutput, calls=%fused_computation.7 | convolution fusion | flops 1074003968 | bytes 9437184 | tf_op jit(solution)/shard_map/dot_general | solution.py:110
  (21 shorter events, 0.3 us)
Async XLA Ops:
  6.5 80.5 %copy-start = (bf16[512,1024]{1,0:T(8,128)(2,1)S(1)}, bf16[512,1024]{1,0:T(8,128)(2,1)}, u32[]{:S(2)}) copy-start(bf16[512,1024]{1,0:T(8,128)(2,1)} %param.13) | copy-start | bytes 3145732
  6.5 71.6 %copy-start.2 = (bf16[1,128,512]{2,1,0:T(8,128)(2,1)S(1)}, bf16[1,128,512]{2,1,0:T(8,128)(2,1)}, u32[]{:S(2)}) copy-start(bf16[1,128,512]{2,1,0:T(8,128)(2,1)} %param.9) | copy-start | bytes 393220
  6.5 66.9 %all-gather.2.cloned.1.call-start = ((), (), s32[]{:S(2)}) async-start(), calls=%async_computation.2 | async-start | bytes 3538944 | tf_op jit(solution)/shard_map/all_gather | solution.py:89
  82.2 19.5 %all-to-all-start = ((bf16[128,4,768]{0,2,1:T(8,128)(2,1)}), bf16[128,4,768]{0,2,1:T(8,128)(2,1)S(1)}, u32[]{:S(2)}, u32[]{:S(2)}) async-start(bf16[128,4,768]{0,2,1:T(8,128)(2,1)} %bitcast.6), calls=%async_computation | async-start | bytes 1572864 | tf_op jit(solution)/shard_map/all_to_all | solution.py:99
  101.7 1.6 %copy-start.1 = (pred[512,512]{0,1:T(8,128)(4,1)S(1)}, pred[512,512]{0,1:T(8,128)(4,1)}, u32[]{:S(2)}) copy-start(pred[512,512]{0,1:T(8,128)(4,1)} %iota_compare_fusion) | copy-start | bytes 786436
  104.5 1.0 copy-start.3
  105.5 5.4 %copy-start.4 = (bf16[2048]{0:T(1024)(128)(2,1)S(1)}, bf16[2048]{0:T(1024)(128)(2,1)}, u32[]{:S(2)}) copy-start(bf16[2048]{0:T(1024)(128)(2,1)} %param.17) | copy-start | bytes 12292
  107.3 11.5 %all-to-all-start.1 = ((bf16[4,128,512]{1,2,0:T(8,128)(2,1)}), bf16[4,128,512]{1,2,0:T(8,128)(2,1)S(1)}, u32[]{:S(2)}, u32[]{:S(2)}) async-start(bf16[4,128,512]{1,2,0:T(8,128)(2,1)} %copy.28), calls=%async_computation.1 | async-start | bytes 1048576 | tf_op jit(solution)/shard_map/all_to_all | solution.py:108
Sparse Core Ops, SparseCore 0:
  9.4 63.9 all-gather.1
where the time goes:
time: 133 us; the launch traced here: 132 us
  waiting for transfers between devices  60.9 us (46%)
  blocking collectives  17.6 us (13%)
  between operations  13.5 us (10%)
  matrix products  12.8 us (10%)
  local copies, waits for them, and re-layouts  10.1 us (8%)
  starting transfers between devices  8.46 us (6%)
  other arithmetic  8.35 us (6%)
    all_gather x1, waiting for transfers between devices, per_device(): lax.all_gather(w_query, 'dp', axis=1, tiled=True)  52.3 us
    all_gather x1, blocking collectives, per_device(): lax.all_gather(rope_turned, 'sp', axis=0, tiled=True)  9.1 us
    all_gather x1, blocking collectives, per_device(): lax.all_gather(latent_norm, 'sp', axis=0, tiled=True)  8.53 us
    all_to_all x1, waiting for transfers between devices, per_device(): lax.all_to_all(attended, 'sp', split_axis=0, concat_axis=1, tiled=True)  7.84 us
    dot_general x1, matrix products, per_device(): jnp.dot(mixed_norm, w_out, preferred_element_type=jnp.float32)  5.47 us
    all_to_all x1, starting transfers between devices, per_device(): lax.all_to_all(queries, 'sp', split_axis=1, concat_axis=0, tiled=True)  4.86 us
    dot_general x1, local copies, waits for them, and re-layouts, per_device(): jnp.dot(query_norm, lax.all_gather(w_query, 'dp', axis=1, tiled=True), pr...  4.68 us
    all_to_all x1, starting transfers between devices, per_device(): lax.all_to_all(attended, 'sp', split_axis=0, concat_axis=1, tiled=True)  3.61 us
  transfers between devices with their start and end apart: 3, of which 2 were waited for; matrix products, arithmetic and copies ran while one was open for 8% of the time, Pallas kernels for 0%

commit v1 on v0

v1 whole, which is shorter than its diff:
```python
import functools

import jax
import jax.numpy as jnp
import numpy as np
from jax import lax
from jax.experimental import pallas as pl
from jax.experimental.pallas import tpu as pltpu
from jax.sharding import PartitionSpec as P

H = 16
NOPE = 128
ROPE = 64
VDIM = 128
HEAD = NOPE + ROPE
MESH = pl.DeviceIdType.MESH
F32 = jnp.float32
BF16 = jnp.bfloat16


def turn_table(length):
    half = ROPE // 2
    inverse = np.float32(10000.0) ** (-np.arange(half, dtype=np.float32) / np.float32(half))
    angles = np.arange(length, dtype=np.float32)[:, None] * inverse[None, :].astype(np.float32)
    angles = angles.astype(np.float64)
    cosine, sine = np.cos(angles), np.sin(angles)
    return np.concatenate([cosine, cosine, sine, sine], axis=1).astype(np.float32)


def spread_matrix(rows, row_start, head):
    g = lax.broadcasted_iota(jnp.int32, (rows, 256), 0) + row_start
    f = lax.broadcasted_iota(jnp.int32, (rows, 256), 1)
    source = jnp.where(f < HEAD, f, jnp.where(f < HEAD + 32, f - 32, f - 96)) + head * HEAD
    sign = jnp.where((f >= HEAD) & (f < HEAD + 32), -1.0, 1.0)
    return jnp.where(g == source, sign, 0.0).astype(BF16)


def rope_matrix():
    r = lax.broadcasted_iota(jnp.int32, (ROPE, 128), 0)
    f = lax.broadcasted_iota(jnp.int32, (ROPE, 128), 1)
    source = jnp.where(f < 64, f, jnp.where(f < 96, f - 32, f - 96))
    sign = jnp.where((f >= 64) & (f < 96), -1.0, 1.0)
    return jnp.where(r == source, sign, 0.0).astype(BF16)


def scaled_rows(values, gain):
    wide = values.astype(F32)
    mean = jnp.mean(wide * wide, axis=-1, keepdims=True)
    return (wide * lax.rsqrt(mean + 1e-05) * gain).astype(BF16)


def kernel(
    geometry,
    q_ref, kv_ref, rope_ref, wq_ref, wkv_ref, wout_ref, table_ref, qg_ref, lg_ref, og_ref,
    out_ref,
    qall, kvall, ropeall, wqall, wkv, wout, table, wp, qn, qs, ks, vs, att_out, att_in, acc,
    local_sem, gat_send, gat_recv, fwd_send, w_send, w_recv, att_send, att_recv,
):
    n, m, X, k, chunks, local_heads = geometry
    Z = m // X
    rows = q_ref.shape[1]
    n_chips = n // 2
    i = lax.axis_index("sp")
    j = lax.axis_index("dp")
    core = lax.rem(i, 2)
    chip = lax.div(i, 2)
    partner = i + 1 - 2 * core
    z = lax.div(j, X)
    x = lax.rem(j, X)
    first = i * k
    owns = (j >= first) & (j < first + k)

    gathered = ((kv_ref.at[0], kvall), (rope_ref.at[0], ropeall), (q_ref.at[0], qall))
    own_copies = [
        pltpu.make_async_copy(src, dst.at[i], local_sem.at[a]) for a, (src, dst) in enumerate(gathered)
    ]
    wq_copy = pltpu.make_async_copy(wq_ref, wqall.at[lax.rem(j, k)], local_sem.at[3])
    wkv_copy = pltpu.make_async_copy(wkv_ref, wkv, local_sem.at[4])
    table_copy = pltpu.make_async_copy(table_ref, table, local_sem.at[5])
    wout_copy = pltpu.make_async_copy(wout_ref, wout, local_sem.at[6])

    @pl.when(owns)
    def _():
        wq_copy.start()

    for copy in own_copies:
        copy.start()
    wkv_copy.start()
    table_copy.start()
    wout_copy.start()

    barrier = pltpu.get_barrier_semaphore()
    for d in range(1, n):
        pl.semaphore_signal(
            barrier, inc=1, device_id={"sp": lax.rem(i + d, n)}, device_id_type=MESH
        )
    sides = ((z < Z - 1, j + X), (z > 0, j - X), (x < X - 1, j + 1), (x > 0, j - 1))
    count = n - 1
    for present, target in sides:
        @pl.when(present)
        def _(target=target):
            pl.semaphore_signal(barrier, inc=1, device_id={"dp": target}, device_id_type=MESH)
        count = count + jnp.where(present, 1, 0)
    pl.semaphore_wait(barrier, count)

    step_rows = wqall.shape[1] // chunks

    def relay_parts(slot, c):
        owner = first + slot
        zo, xo = lax.div(owner, X), lax.rem(owner, X)
        part = wqall.at[slot, pl.ds(c * step_rows, step_rows)]
        in_column = x == xo
        conditions = (
            in_column & (z >= zo) & (z < Z - 1),
            in_column & (z <= zo) & (z > 0),
            (x >= xo) & (x < X - 1),
            (x <= xo) & (x > 0),
        )
        copies = [
            pltpu.make_async_remote_copy(
                src_ref=part, dst_ref=part,
                send_sem=w_send.at[side, slot, c], recv_sem=w_recv.at[slot, c],
                device_id={"dp": sides[side][1]}, device_id_type=MESH,
            )
            for side in range(4)
        ]
        return owner, conditions, copies

    def relay(slot, c):
        owner, conditions, copies = relay_parts(slot, c)

        @pl.when(owner != j)
        def _():
            copies[0].wait_recv()

        for condition, copy in zip(conditions, copies):
            @pl.when(condition)
            def _(copy=copy):
                copy.start()

    def relay_finish(slot, c):
        _, conditions, copies = relay_parts(slot, c)
        for condition, copy in zip(conditions, copies):
            @pl.when(condition)
            def _(copy=copy):
                copy.wait_send()

    if k == X:
        columns = [lax.rem(x + t, k) for t in range(k)]
        events = []
        for c in range(chunks + k - 1):
            for t in range(k):
                if 0 <= c - t < chunks:
                    events.append((columns[t], c - t))
    else:
        events = [(slot, c) for c in range(chunks) for slot in range(k)]
    events_left = list(events)

    def relay_some(number):
        for _ in range(min(number, len(events_left))):
            relay(*events_left.pop(0))

    def gather_copy(a, slot, sem, target):
        dst = gathered[a][1]
        return pltpu.make_async_remote_copy(
            src_ref=dst.at[slot], dst_ref=dst.at[slot],
            send_sem=sem, recv_sem=gat_recv.at[a, slot],
            device_id={"sp": target}, device_id_type=MESH,
        )

    sends = []

    @pl.when(owns)
    def _():
        wq_copy.wait()

    for a in range(3):
        own_copies[a].wait()
        for d in range(1, n_chips):
            target = 2 * lax.rem(chip + d, n_chips) + core
            sends.append(gather_copy(a, i, gat_send.at[a, d], target))
            sends[-1].start()
    for a in range(3):
        sends.append(gather_copy(a, i, gat_send.at[a, 0], partner))
        sends[-1].start()

    def far_slot(d):
        return 2 * lax.rem(chip + n_chips - d, n_chips) + core

    def forward(a, d):
        slot = far_slot(d)
        copy = gather_copy(a, slot, fwd_send.at[a, d - 1], partner)
        copy.wait_recv()
        copy.start()
        sends.append(copy)

    def arrive(a, slot):
        gather_copy(a, slot, gat_send.at[a, 0], partner).wait_recv()

    lane = lax.broadcasted_iota(jnp.int32, (rows, 128), 1)
    latent_gain = lg_ref[...].astype(F32)
    query_gain = qg_ref[...].astype(F32)
    turner = rope_matrix()

    def keyval(slot):
        at = pl.ds(pl.multiple_of(slot * rows, rows), rows)
        both = jnp.dot(
            scaled_rows(kvall[slot], latent_gain), wkv[...], preferred_element_type=F32
        ).astype(BF16)
        pair = jnp.dot(ropeall[slot], turner, preferred_element_type=F32) * table[at, :]
        pair = pair + pltpu.roll(pair, 64, 1)
        turned = jnp.where(lane < 64, pair, 0.0).astype(BF16)
        for h in range(local_heads):
            base = h * (NOPE + VDIM)
            ks[h, at, 0:NOPE] = both[:, base:base + NOPE]
            ks[h, at, NOPE:256] = turned
            vs[h, at, :] = both[:, base + NOPE:base + NOPE + VDIM]

    def query_rows(slot):
        at = pl.ds(pl.multiple_of(slot * rows, rows), rows)
        qn[at, :] = scaled_rows(qall[slot], query_gain)

    relay_some(k + 1)
    wkv_copy.wait()
    table_copy.wait()
    keyval(i)
    relay_some(1)
    query_rows(i)
    relay_some(1)
    arrive(0, partner)
    arrive(1, partner)
    keyval(partner)
    relay_some(1)
    for d in range(1, n_chips):
        forward(0, d)
        forward(1, d)
        keyval(far_slot(d))
        relay_some(1)
    arrive(2, partner)
    query_rows(partner)
    relay_some(2)
    for d in range(1, n_chips):
        other = far_slot(d) + 1 - 2 * core
        arrive(0, other)
        arrive(1, other)
        keyval(other)
        relay_some(2)
    for d in range(1, n_chips):
        forward(2, d)
        query_rows(far_slot(d))
        relay_some(2)
    for d in range(1, n_chips):
        other = far_slot(d) + 1 - 2 * core
        arrive(2, other)
        query_rows(other)
    relay_some(len(events_left))

    width = wqall.shape[2]
    for h in range(local_heads):
        total = None
        for s in range(k):
            if (s + 1) * width <= h * HEAD or s * width >= (h + 1) * HEAD:
                continue
            term = jnp.dot(
                wqall[s], spread_matrix(width, s * width, h), preferred_element_type=F32
            )
            total = term if total is None else total + term
        wp[h] = total.astype(BF16)
        raw = jnp.dot(qn[...], wp[h], preferred_element_type=F32)
        qs[h, :, 0:NOPE] = raw[:, 0:NOPE].astype(BF16)
        pair = raw[:, NOPE:256] * table[...]
        qs[h, :, NOPE:256] = (pair + pltpu.roll(pair, 64, 1)).astype(BF16)

    power = HEAD ** (-0.5) * float(np.log2(np.e))
    causal = lax.broadcasted_iota(jnp.int32, (rows, rows), 1) <= lax.broadcasted_iota(
        jnp.int32, (rows, rows), 0
    )

    def attend(b):
        stop = (b + 1) * rows
        for h in range(local_heads):
            scores = lax.dot_general(
                qs[h, b * rows:stop, :], ks[h, 0:stop, :], (((1,), (1,)), ((), ())),
                preferred_element_type=F32,
            )
            last = jnp.where(causal, scores[:, b * rows:], -jnp.inf)
            if b:
                scores = jnp.concatenate([scores[:, :b * rows], last], axis=1)
            else:
                scores = last
            top = jnp.max(scores, axis=-1, keepdims=True)
            weights = jnp.exp2((scores - top) * power)
            row_total = jnp.sum(weights, axis=-1, keepdims=True)
            summed = jnp.dot(weights.astype(BF16), vs[h, 0:stop, :], preferred_element_type=F32)
            att_out[b, :, h * VDIM:(h + 1) * VDIM] = (summed / row_total).astype(BF16)

    def att_copy(b):
        return pltpu.make_async_remote_copy(
            src_ref=att_out.at[b], dst_ref=att_in.at[i],
            send_sem=att_send.at[b], recv_sem=att_recv.at[i],
            device_id={"sp": b}, device_id_type=MESH,
        )

    for b in range(n):
        @pl.when(chip != b // 2)
        def _(b=b):
            attend(b)
            att_copy(b).start()
    for b in range(n):
        @pl.when(partner == b)
        def _(b=b):
            attend(b)
            att_copy(b).start()
    for b in range(n):
        @pl.when(i == b)
        def _(b=b):
            attend(b)

    group = local_heads * VDIM
    wout_copy.wait()
    squares = None
    order = [partner]
    for d in range(1, n_chips):
        order += [far_slot(d), far_slot(d) + 1 - 2 * core]
    for t, s in enumerate([i] + order):
        if t:
            pltpu.make_async_remote_copy(
                src_ref=att_in.at[s], dst_ref=att_in.at[s],
                send_sem=att_send.at[0], recv_sem=att_recv.at[s],
                device_id={"sp": partner}, device_id_type=MESH,
            ).wait_recv()
            values = att_in[s].astype(F32)
        else:
            values = att_out[i].astype(F32)
        at = pl.ds(pl.multiple_of(s * group, group), group)
        square = jnp.sum(values * values, axis=-1, keepdims=True)
        squares = square if squares is None else squares + square
        scaled = (values * og_ref[s].astype(F32)).astype(BF16)
        term = jnp.dot(scaled, wout[at, :], preferred_element_type=F32)
        if t == 0:
            acc[...] = term
        elif t < n - 1:
            acc[...] += term
        else:
            factor = lax.rsqrt(squares / (n * group) + 1e-05)
            out_ref[0] = ((acc[...] + term) * factor).astype(BF16)

    for copy in sends:
        copy.wait_send()
    for event in events:
        relay_finish(*event)
    for b in range(n):
        @pl.when(i != b)
        def _(b=b):
            att_copy(b).wait_send()


def x_size(mesh):
    row = mesh.devices[0]
    places = [getattr(device, "coords", None) for device in row]
    if any(place is None for place in places):
        return 1
    return len({place[0] for place in places})


def per_device(
    mesh, q_latent, kv_latent, rope_key, w_query, w_keyval, w_out, query_gain, latent_gain, out_gain
):
    n, m = mesh.shape["sp"], mesh.shape["dp"]
    rows = q_latent.shape[1]
    length = n * rows
    rank = q_latent.shape[2]
    width = w_query.shape[1]
    local_heads = H // n
    k = local_heads * HEAD // width
    chunks = 8
    dim = w_out.shape[1]
    group = local_heads * VDIM
    table = jnp.asarray(turn_table(length))
    geometry = (n, m, x_size(mesh), k, chunks, local_heads)
    any_spec = pl.BlockSpec(memory_space=pl.ANY)
    vmem_spec = pl.BlockSpec(memory_space=pltpu.VMEM)
    dma = pltpu.SemaphoreType.DMA
    return pl.pallas_call(
        functools.partial(kernel, geometry),
        out_shape=jax.ShapeDtypeStruct((1, rows, dim), BF16),
        in_specs=[any_spec] * 7 + [vmem_spec] * 3,
        out_specs=vmem_spec,
        scratch_shapes=[
            pltpu.VMEM((n, rows, rank), BF16),
            pltpu.VMEM((n, rows, kv_latent.shape[2]), BF16),
            pltpu.VMEM((n, rows, ROPE), BF16),
            pltpu.VMEM((k, rank, width), BF16),
            pltpu.VMEM(w_keyval.shape, BF16),
            pltpu.VMEM(w_out.shape, BF16),
            pltpu.VMEM((length, 128), F32),
            pltpu.VMEM((local_heads, rank, 256), BF16),
            pltpu.VMEM((length, rank), BF16),
            pltpu.VMEM((local_heads, length, 256), BF16),
            pltpu.VMEM((local_heads, length, 256), BF16),
            pltpu.VMEM((local_heads, length, VDIM), BF16),
            pltpu.VMEM((n, rows, group), BF16),
            pltpu.VMEM((n, rows, group), BF16),
            pltpu.VMEM((rows, dim), F32),
            dma((7,)),
            dma((3, n // 2)),
            dma((3, n)),
            dma((3, n // 2)),
            dma((4, k, chunks)),
            dma((k, chunks)),
            dma((n,)),
            dma((n,)),
        ],
        compiler_params=pltpu.CompilerParams(
            collective_id=0, has_side_effects=True, vmem_limit_bytes=56 * 1024 * 1024
        ),
    )(
        q_latent, kv_latent, rope_key, w_query, w_keyval, w_out, table,
        query_gain.reshape(1, -1), latent_gain.reshape(1, -1),
        out_gain.reshape(n, 1, group),
    )


def solution(mesh):
    in_specs = (
        P("dp", "sp", None),
        P("dp", "sp", None),
        P("dp", "sp", None),
        P(None, "dp"),
        P(None, "sp"),
        P(),
        P(),
        P(),
        P(),
    )
    return jax.shard_map(
        functools.partial(per_device, mesh), mesh=mesh, in_specs=in_specs,
        out_specs=P("dp", "sp", None), check_vma=False,
    )
```

time: 133 us -> 47.8 us (0.36)
  waiting for transfers between devices: 60.9 us -> 0 us
  Pallas kernels: 0 us -> 40.3 us
  blocking collectives: 17.6 us -> 0 us
  between operations: 13.5 us -> 0.01 us
  matrix products: 12.8 us -> 0 us
  starting transfers between devices: 8.46 us -> 0 us
  other arithmetic: 8.35 us -> 0 us
  local copies, waits for them, and re-layouts: 10.1 us -> 7.12 us
    all_gather x1 -> x0, waiting for transfers between devices: 52.3 us -> none  [per_device(): lax.all_gather(w_query, 'dp', axis=1, tiled=True)]
    pallas_call x0 -> x1, Pallas kernels: none -> 40.3 us  [per_device(): pl.pallas_call(functools.partial(kernel, geometry), out_shape=jax.ShapeDt...]
    all_gather x2 -> x0, blocking collectives: 17.6 us -> none  [the longest x1 9.1 us: per_device(): lax.all_gather(rope_turned, 'sp', axis=0, tiled=True)]
    dot_general x6 -> x0, matrix products: 12.8 us -> none  [the longest x1 5.47 us: per_device(): jnp.dot(mixed_norm, w_out, preferred_element_type=jnp.float32)]
    all_to_all x2 -> x0, starting transfers between devices: 8.46 us -> none  [the longest x1 4.86 us: per_device(): lax.all_to_all(queries, 'sp', split_axis=1, concat_axis=0, tiled=True)]
    all_to_all x2 -> x0, waiting for transfers between devices: 7.85 us -> none  [the longest x1 7.84 us: per_device(): lax.all_to_all(attended, 'sp', split_axis=0, concat_axis=1, tiled=True)]
    dot_general x1 -> x0, local copies, waits for them, and re-layouts: 4.68 us -> none  [per_device(): jnp.dot(query_norm, lax.all_gather(w_query, 'dp', axis=1, tiled=True), pr...]
    convert_element_type x7 -> x0, other arithmetic: 3.45 us -> none  [the longest x3 1.37 us: normalize(): gain_vector.astype(jnp.float32)]
  transfers between devices with their start and end apart: 3 -> 0, of which waited for: 2 -> 0; matrix products, arithmetic and copies ran while one was open for 8% -> 0% of each run, Pallas kernels for 0% -> 0%
where the time goes in v1:
time: 47.8 us; the launch traced here: 47.4 us
  Pallas kernels  40.3 us (84%)
  local copies, waits for them, and re-layouts  7.12 us (15%)
    pallas_call x1, Pallas kernels, per_device(): pl.pallas_call(functools.partial(kernel, geometry), out_shape=jax.ShapeDt...  40.3 us
    unnamed x2, local copies, waits for them, and re-layouts  3.31 us
    reshape x1, local copies, waits for them, and re-layouts, per_device(): out_gain.reshape(n, 1, group)  1.29 us
    reshape x1, local copies, waits for them, and re-layouts, per_device(): query_gain.reshape(1, -1)  1.26 us
    reshape x1, local copies, waits for them, and re-layouts, per_device(): latent_gain.reshape(1, -1)  1.26 us

profile of v1, /device:TPU:1, one launch (start us, length us, event | category | flops | bytes accessed | tf_op | source)
XLA Modules:
  0.0 47.4 jit_solution(11754632087461182065)
XLA Ops:
  0.0 1.3 %reshape.9.qg_ref = bf16[1,512]{1,0:T(2,128)(2,1)} reshape(bf16[512]{0:T(512)(128)(2,1)} %param.16) | data formatting | bytes 2048 | tf_op jit(solution)/shard_map/reshape | solution.py:419
  1.3 1.3 %reshape.10.lg_ref = bf16[1,512]{1,0:T(2,128)(2,1)} reshape(bf16[512]{0:T(512)(128)(2,1)} %param.17) | data formatting | bytes 2048 | tf_op jit(solution)/shard_map/reshape | solution.py:419
  2.5 1.3 %reshape.12.og_ref = bf16[4,1,512]{2,1,0:T(2,128)(2,1)} reshape(bf16[2048]{0:T(1024)(128)(2,1)} %param.18) | data formatting | bytes 8192 | tf_op jit(solution)/shard_map/reshape | solution.py:420
  3.8 1.4 %copy.12.rope_ref = bf16[1,128,64]{2,1,0:T(8,128)(2,1)} copy(bf16[1,128,64]{1,2,0:T(8,128)(2,1)} %param.12) | data formatting | bytes 32768 | tf_op args[2]
  5.2 40.3 %shard_map.100 = bf16[1,128,2048]{2,1,0:T(8,128)(2,1)} custom-call(bf16[1,128,512]{2,1,0:T(8,128)(2,1)} %q_ref.1, bf16[1,128,512]{2,1,0:T(8,128)(2,1)} %kv_ref.1, bf16[1,128,64]{2,1,0:T(8,128)(2,1)} %copy.12.rope_ref, bf16[512,384]{1,0:T(8,128)(2,1)} %wq_ref.1, bf16[512,1024]{1,0:T(8,128)(2,1)} %wkv_ref.1, bf16[2048,2048]{1,0:T(8,128)(2,1)} %wout_ref.1, ...), custom_call_target="tpu_custom_call" | custom-call | tf_op jit(solution)/shard_map/pallas_call | solution.py:384
  45.5 1.9 %copy.15 = bf16[1,128,2048]{2,1,0:T(8,128)(2,1)} copy(bf16[1,128,2048]{2,1,0:T(8,128)(2,1)} %shard_map.100) | data formatting | bytes 1048576

commit v2 on v1

--- a/solution.py
+++ b/solution.py
@@ -53,10 +53,13 @@
     geometry,
     q_ref, kv_ref, rope_ref, wq_ref, wkv_ref, wout_ref, table_ref, qg_ref, lg_ref, og_ref,
     out_ref,
-    qall, kvall, ropeall, wqall, wkv, wout, table, wp, qn, qs, ks, vs, att_out, att_in, acc,
+    qall, kvall, ropeall, wqall, wkv, wout, table, spread, qn, qs, ks, vs, att_out, att_in, acc,
+    out_gain,
     local_sem, gat_send, gat_recv, fwd_send, w_send, w_recv, att_send, att_recv,
 ):
-    n, m, X, k, chunks, local_heads = geometry
+    n, m, X, k, chunks, local_heads, groups = geometry
+    per_group = local_heads // groups
+    width = wqall.shape[2]
     Z = m // X
     rows = q_ref.shape[1]
     n_chips = n // 2
@@ -88,6 +91,17 @@
     wkv_copy.start()
     table_copy.start()
     wout_copy.start()
+
+    turner = rope_matrix()
+    latent_gain = lg_ref[...].astype(F32).reshape(1, -1)
+    query_gain = qg_ref[...].astype(F32).reshape(1, -1)
+    group = local_heads * VDIM
+    every_gain = og_ref[...].astype(F32).reshape(1, -1)
+    for s in range(n):
+        out_gain[s] = every_gain[:, s * group:(s + 1) * group]
+    if groups > 1:
+        for h in range(per_group):
+            spread[h] = spread_matrix(width, 0, h)
 
     barrier = pltpu.get_barrier_semaphore()
     for d in range(1, n):
@@ -145,16 +159,13 @@
             def _(copy=copy):
                 copy.wait_send()
 
-    if k == X:
+    if groups > 1:
         columns = [lax.rem(x + t, k) for t in range(k)]
-        events = []
-        for c in range(chunks + k - 1):
-            for t in range(k):
-                if 0 <= c - t < chunks:
-                    events.append((columns[t], c - t))
+        events = [[(column, c) for c in range(chunks)] for column in columns]
     else:
-        events = [(slot, c) for c in range(chunks) for slot in range(k)]
-    events_left = list(events)
+        columns = [0]
+        events = [[(slot, c) for c in range(chunks) for slot in range(k)]]
+    events_left = list(events[0])
 
     def relay_some(number):
         for _ in range(min(number, len(events_left))):
@@ -198,16 +209,15 @@
         gather_copy(a, slot, gat_send.at[a, 0], partner).wait_recv()
 
     lane = lax.broadcasted_iota(jnp.int32, (rows, 128), 1)
-    latent_gain = lg_ref[...].astype(F32)
-    query_gain = qg_ref[...].astype(F32)
-    turner = rope_matrix()
 
     def keyval(slot):
         at = pl.ds(pl.multiple_of(slot * rows, rows), rows)
         both = jnp.dot(
             scaled_rows(kvall[slot], latent_gain), wkv[...], preferred_element_type=F32
         ).astype(BF16)
-        pair = jnp.dot(ropeall[slot], turner, preferred_element_type=F32) * table[at, :]
+        pair = lax.dot_general(
+            ropeall[slot], turner, (((0,), (0,)), ((), ())), preferred_element_type=F32
+        ) * table[at, :]
         pair = pair + pltpu.roll(pair, 64, 1)
         turned = jnp.where(lane < 64, pair, 0.0).astype(BF16)
         for h in range(local_heads):
@@ -255,30 +265,37 @@
         query_rows(other)
     relay_some(len(events_left))
 
-    width = wqall.shape[2]
-    for h in range(local_heads):
-        total = None
-        for s in range(k):
-            if (s + 1) * width <= h * HEAD or s * width >= (h + 1) * HEAD:
-                continue
-            term = jnp.dot(
-                wqall[s], spread_matrix(width, s * width, h), preferred_element_type=F32
-            )
-            total = term if total is None else total + term
-        wp[h] = total.astype(BF16)
-        raw = jnp.dot(qn[...], wp[h], preferred_element_type=F32)
-        qs[h, :, 0:NOPE] = raw[:, 0:NOPE].astype(BF16)
-        pair = raw[:, NOPE:256] * table[...]
-        qs[h, :, NOPE:256] = (pair + pltpu.roll(pair, 64, 1)).astype(BF16)
+    def raw_queries(slot, hh):
+        if groups > 1:
+            total = jnp.dot(wqall[slot], spread[hh], preferred_element_type=F32)
+        else:
+            total = None
+            for s in range(k):
+                if (s + 1) * width <= hh * HEAD or s * width >= (hh + 1) * HEAD:
+                    continue
+                term = jnp.dot(
+                    wqall[s], spread_matrix(width, s * width, hh), preferred_element_type=F32
+                )
+                total = term if total is None else total + term
+        return jnp.dot(qn[...], total.astype(BF16), preferred_element_type=F32)
+
+    def queries(slot):
+        for hh in range(per_group):
+            h = slot * per_group + hh
+            raw = raw_queries(slot, hh)
+            qs[h, :, 0:NOPE] = raw[:, 0:NOPE].astype(BF16)
+            pair = raw[:, NOPE:256] * table[...]
+            qs[h, :, NOPE:256] = (pair + pltpu.roll(pair, 64, 1)).astype(BF16)
 
     power = HEAD ** (-0.5) * float(np.log2(np.e))
     causal = lax.broadcasted_iota(jnp.int32, (rows, rows), 1) <= lax.broadcasted_iota(
         jnp.int32, (rows, rows), 0
     )
 
-    def attend(b):
+    def attend(b, slot):
         stop = (b + 1) * rows
-        for h in range(local_heads):
+        for hh in range(per_group):
+            h = slot * per_group + hh
             scores = lax.dot_general(
                 qs[h, b * rows:stop, :], ks[h, 0:stop, :], (((1,), (1,)), ((), ())),
                 preferred_element_type=F32,
@@ -292,50 +309,55 @@
             weights = jnp.exp2((scores - top) * power)
             row_total = jnp.sum(weights, axis=-1, keepdims=True)
             summed = jnp.dot(weights.astype(BF16), vs[h, 0:stop, :], preferred_element_type=F32)
-            att_out[b, :, h * VDIM:(h + 1) * VDIM] = (summed / row_total).astype(BF16)
-
-    def att_copy(b):
+            att_out[b, slot, :, hh * VDIM:(hh + 1) * VDIM] = (summed / row_total).astype(BF16)
+
+    def att_copy(b, slot):
         return pltpu.make_async_remote_copy(
-            src_ref=att_out.at[b], dst_ref=att_in.at[i],
-            send_sem=att_send.at[b], recv_sem=att_recv.at[i],
+            src_ref=att_out.at[b, slot], dst_ref=att_in.at[i, slot],
+            send_sem=att_send.at[b, slot], recv_sem=att_recv.at[i, slot],
             device_id={"sp": b}, device_id_type=MESH,
         )
 
-    for b in range(n):
-        @pl.when(chip != b // 2)
-        def _(b=b):
-            attend(b)
-            att_copy(b).start()
-    for b in range(n):
-        @pl.when(partner == b)
-        def _(b=b):
-            attend(b)
-            att_copy(b).start()
-    for b in range(n):
-        @pl.when(i == b)
-        def _(b=b):
-            attend(b)
-
-    group = local_heads * VDIM
+    for t, slot in enumerate(columns):
+        if t:
+            for event in events[t]:
+                relay(*event)
+        queries(slot)
+        for b in range(n):
+            @pl.when(chip != b // 2)
+            def _(b=b):
+                attend(b, slot)
+                att_copy(b, slot).start()
+        for b in range(n):
+            @pl.when(partner == b)
+            def _(b=b):
+                attend(b, slot)
+                att_copy(b, slot).start()
+        for b in range(n):
+            @pl.when(i == b)
+            def _(b=b):
+                attend(b, slot)
+
     wout_copy.wait()
     squares = None
     order = [partner]
     for d in range(1, n_chips):
         order += [far_slot(d), far_slot(d) + 1 - 2 * core]
     for t, s in enumerate([i] + order):
+        source = att_out
         if t:
-            pltpu.make_async_remote_copy(
-                src_ref=att_in.at[s], dst_ref=att_in.at[s],
-                send_sem=att_send.at[0], recv_sem=att_recv.at[s],
-                device_id={"sp": partner}, device_id_type=MESH,
-            ).wait_recv()
-            values = att_in[s].astype(F32)
-        else:
-            values = att_out[i].astype(F32)
+            source = att_in
+            for slot in range(groups):
+                pltpu.make_async_remote_copy(
+                    src_ref=att_in.at[s, slot], dst_ref=att_in.at[s, slot],
+                    send_sem=att_send.at[0, slot], recv_sem=att_recv.at[s, slot],
+                    device_id={"sp": partner}, device_id_type=MESH,
+                ).wait_recv()
+        values = jnp.concatenate([source[s, slot] for slot in range(groups)], axis=1).astype(F32)
         at = pl.ds(pl.multiple_of(s * group, group), group)
         square = jnp.sum(values * values, axis=-1, keepdims=True)
         squares = square if squares is None else squares + square
-        scaled = (values * og_ref[s].astype(F32)).astype(BF16)
+        scaled = (values * out_gain[s]).astype(BF16)
         term = jnp.dot(scaled, wout[at, :], preferred_element_type=F32)
         if t == 0:
             acc[...] = term
@@ -347,12 +369,13 @@
 
     for copy in sends:
         copy.wait_send()
-    for event in events:
+    for event in sum(events, []):
         relay_finish(*event)
     for b in range(n):
         @pl.when(i != b)
         def _(b=b):
-            att_copy(b).wait_send()
+            for slot in range(groups):
+                att_copy(b, slot).wait_send()
 
 
 def x_size(mesh):
@@ -373,11 +396,13 @@
     width = w_query.shape[1]
     local_heads = H // n
     k = local_heads * HEAD // width
-    chunks = 8
+    chunks = 16
+    columns = x_size(mesh)
+    groups = k if k == columns == 2 and width % HEAD == 0 else 1
     dim = w_out.shape[1]
     group = local_heads * VDIM
     table = jnp.asarray(turn_table(length))
-    geometry = (n, m, x_size(mesh), k, chunks, local_heads)
+    geometry = (n, m, columns, k, chunks, local_heads, groups)
     any_spec = pl.BlockSpec(memory_space=pl.ANY)
     vmem_spec = pl.BlockSpec(memory_space=pltpu.VMEM)
     dma = pltpu.SemaphoreType.DMA
@@ -389,35 +414,35 @@
         scratch_shapes=[
             pltpu.VMEM((n, rows, rank), BF16),
             pltpu.VMEM((n, rows, kv_latent.shape[2]), BF16),
-            pltpu.VMEM((n, rows, ROPE), BF16),
+            pltpu.VMEM((n, ROPE, rows), BF16),
             pltpu.VMEM((k, rank, width), BF16),
             pltpu.VMEM(w_keyval.shape, BF16),
             pltpu.VMEM(w_out.shape, BF16),
             pltpu.VMEM((length, 128), F32),
-            pltpu.VMEM((local_heads, rank, 256), BF16),
+            pltpu.VMEM((local_heads // groups, width, 256), BF16),
             pltpu.VMEM((length, rank), BF16),
             pltpu.VMEM((local_heads, length, 256), BF16),
             pltpu.VMEM((local_heads, length, 256), BF16),
             pltpu.VMEM((local_heads, length, VDIM), BF16),
-            pltpu.VMEM((n, rows, group), BF16),
-            pltpu.VMEM((n, rows, group), BF16),
+            pltpu.VMEM((n, groups, rows, group // groups), BF16),
+            pltpu.VMEM((n, groups, rows, group // groups), BF16),
             pltpu.VMEM((rows, dim), F32),
+            pltpu.VMEM((n, 1, group), F32),
             dma((7,)),
             dma((3, n // 2)),
             dma((3, n)),
             dma((3, n // 2)),
             dma((4, k, chunks)),
             dma((k, chunks)),
-            dma((n,)),
-            dma((n,)),
+            dma((n, groups)),
+            dma((n, groups)),
         ],
         compiler_params=pltpu.CompilerParams(
             collective_id=0, has_side_effects=True, vmem_limit_bytes=56 * 1024 * 1024
         ),
     )(
-        q_latent, kv_latent, rope_key, w_query, w_keyval, w_out, table,
-        query_gain.reshape(1, -1), latent_gain.reshape(1, -1),
-        out_gain.reshape(n, 1, group),
+        q_latent, kv_latent, jnp.swapaxes(rope_key, 1, 2), w_query, w_keyval, w_out, table,
+        query_gain, latent_gain, out_gain,
     )
 
 

time: 47.8 us -> 38.8 us (0.81)
  local copies, waits for them, and re-layouts: 7.12 us -> 1.88 us
  Pallas kernels: 40.3 us -> 36.7 us
    reshape x3 -> x0, local copies, waits for them, and re-layouts: 3.81 us -> none  [the longest x1 1.29 us: per_device(): out_gain.reshape(n, 1, group)]
    pallas_call x1, Pallas kernels: 40.3 us -> 36.7 us  [per_device(): pl.pallas_call(functools.partial(kernel, geometry), out_shape=jax.ShapeDt...]
    unnamed x2 -> x1, local copies, waits for them, and re-layouts: 3.31 us -> 1.88 us
where the time goes in v2:
time: 38.8 us; the launch traced here: 38.6 us
  Pallas kernels  36.7 us (95%)
  local copies, waits for them, and re-layouts  1.88 us (5%)
    pallas_call x1, Pallas kernels, per_device(): pl.pallas_call(functools.partial(kernel, geometry), out_shape=jax.ShapeDt...  36.7 us
    unnamed x1, local copies, waits for them, and re-layouts  1.88 us

profile of v2, /device:TPU:1, one launch (start us, length us, event | category | flops | bytes accessed | tf_op | source)
XLA Modules:
  0.0 38.6 jit_solution(18350265653516186925)
XLA Ops:
  0.0 36.7 %shard_map.100 = bf16[1,128,2048]{2,1,0:T(8,128)(2,1)} custom-call(bf16[1,128,512]{2,1,0:T(8,128)(2,1)} %q_ref.1, bf16[1,128,512]{2,1,0:T(8,128)(2,1)} %kv_ref.1, bf16[1,64,128]{2,1,0:T(8,128)(2,1)} %bitcast.1, bf16[512,384]{1,0:T(8,128)(2,1)} %wq_ref.1, bf16[512,1024]{1,0:T(8,128)(2,1)} %wkv_ref.1, bf16[2048,2048]{1,0:T(8,128)(2,1)} %wout_ref.1, ...), custom_call_target="tpu_custom_call" | custom-call | tf_op jit(solution)/shard_map/pallas_call | solution.py:409
  36.7 1.9 %copy.12 = bf16[1,128,2048]{2,1,0:T(8,128)(2,1)} copy(bf16[1,128,2048]{2,1,0:T(8,128)(2,1)} %shard_map.100) | data formatting | bytes 1048576

commit v3 on v2

--- a/solution.py
+++ b/solution.py
@@ -323,20 +323,20 @@
             for event in events[t]:
                 relay(*event)
         queries(slot)
-        for b in range(n):
-            @pl.when(chip != b // 2)
-            def _(b=b):
-                attend(b, slot)
-                att_copy(b, slot).start()
-        for b in range(n):
-            @pl.when(partner == b)
-            def _(b=b):
-                attend(b, slot)
-                att_copy(b, slot).start()
-        for b in range(n):
-            @pl.when(i == b)
-            def _(b=b):
-                attend(b, slot)
+        for c in range(n_chips):
+            @pl.when(chip != c)
+            def _(c=c):
+                for b in (2 * c, 2 * c + 1):
+                    attend(b, slot)
+                    att_copy(b, slot).start()
+    for c in range(n_chips):
+        @pl.when(chip == c)
+        def _(c=c):
+            for slot in columns:
+                for b in (2 * c, 2 * c + 1):
+                    attend(b, slot)
+    for slot in columns:
+        att_copy(partner, slot).start()
 
     wout_copy.wait()
     squares = None

time: 38.8 us -> 37.6 us (0.969)
  Pallas kernels: 36.7 us -> 35.3 us
    pallas_call x1, Pallas kernels: 36.7 us -> 35.3 us  [per_device(): pl.pallas_call(functools.partial(kernel, geometry), out_shape=jax.ShapeDt...]
where the time goes in v3:
time: 37.6 us; the launch traced here: 37.2 us
  Pallas kernels  35.3 us (94%)
  local copies, waits for them, and re-layouts  1.88 us (5%)
    pallas_call x1, Pallas kernels, per_device(): pl.pallas_call(functools.partial(kernel, geometry), out_shape=jax.ShapeDt...  35.3 us
    unnamed x1, local copies, waits for them, and re-layouts  1.88 us

profile of v3, /device:TPU:1, one launch (start us, length us, event | category | flops | bytes accessed | tf_op | source)
XLA Modules:
  0.0 37.2 jit_solution(13719510512092117200)
XLA Ops:
  0.0 35.3 %shard_map.100 = bf16[1,128,2048]{2,1,0:T(8,128)(2,1)} custom-call(bf16[1,128,512]{2,1,0:T(8,128)(2,1)} %q_ref.1, bf16[1,128,512]{2,1,0:T(8,128)(2,1)} %kv_ref.1, bf16[1,64,128]{2,1,0:T(8,128)(2,1)} %bitcast.1, bf16[512,384]{1,0:T(8,128)(2,1)} %wq_ref.1, bf16[512,1024]{1,0:T(8,128)(2,1)} %wkv_ref.1, bf16[2048,2048]{1,0:T(8,128)(2,1)} %wout_ref.1, ...), custom_call_target="tpu_custom_call" | custom-call | tf_op jit(solution)/shard_map/pallas_call | solution.py:409
  35.3 1.9 %copy.12 = bf16[1,128,2048]{2,1,0:T(8,128)(2,1)} copy(bf16[1,128,2048]{2,1,0:T(8,128)(2,1)} %shard_map.100) | data formatting | bytes 1048576
